TPU v7x, 32 devices: a whole 2x2x4 slice. The times are simulated.
32 devices in a mesh: ep: 8 (over z, core), tp: 4 (over y, x).
Axes of the slice: x: 2, y: 2, z: 4, core: 2. Of those that a mesh axis runs over, the one named last changes fastest.
Arguments:
- mixer_rows: bfloat16 [2048, 2048], P('ep'), may hold values from -8 to 8
- mixer_gain: float32 [2048], replicated, may hold values from 0.1 to 1.9
- w_query: bfloat16 [2048, 1024], P(None, 'tp'), may hold values from -0.125 to 0.125
- w_key: bfloat16 [2048, 1024], P(None, 'tp'), may hold values from -0.125 to 0.125
- w_value: bfloat16 [2048, 1024], P(None, 'tp'), may hold values from -0.125 to 0.125
- key_shift: float32 [16, 2048], P('tp'), may hold values from -14 to 0
- w_out: bfloat16 [1024, 2048], P(None, 'tp'), may hold values from -0.75 to 0.75
- expert_rows: bfloat16 [1024, 2048], P('ep'), may hold values from -6 to 6
- expert_gain: float32 [2048], replicated, may hold values from 0.1 to 1.9
- routes: int32 [1024, 4], P('ep'), may hold values from 0 to 7, all different within a row; in each aligned block of 128 rows (0 to 127, 128 to 255, ...) at most 128 rows name the same one
- route_weight: float32 [1024, 4], P('ep'), may hold values from 0.05 to 0.6
- w_gate: bfloat16 [8, 2048, 2048], P('ep', None, 'tp'), may hold values from -0.25 to 0.25
- w_up: bfloat16 [8, 2048, 2048], P('ep', None, 'tp'), may hold values from -0.25 to 0.25
- w_down: bfloat16 [8, 2048, 2048], P('ep', None, 'tp'), may hold values from -0.0625 to 0.0625
Outputs:
- mixer_out: bfloat16 [2048, 2048], P('ep', 'tp')
- expert_out: bfloat16 [1024, 2048], P('ep', 'tp')
Inputs may be any that keep to these rules, and one draw needn't show every extreme that they name: `routes`: each row names 4 different experts. In each aligned block of 128 rows no expert is named by more than 128 rows, and in every draw some block names some expert exactly 128 times.
All inputs are finite; a program needn't handle non-finite values.
Results may differ from a plain program's by a relative error of at most 0.0073.
Values may be sent and summed in bfloat16 or wider, within the bound.
No kernel may reach another device: no remote copies, remote signals or barrier semaphores. Data moves between devices by JAX's collectives and lax.ppermute only.
A program may use at most 64 MiB of HBM per device.

v0:
```python
import jax
import jax.numpy as jnp
from jax import lax
from jax.sharding import PartitionSpec as P

norm_eps = 1e-06
glu_limit = 7.0
glu_alpha = 1.702


def rms_scale(source, scaling):
    floats = source.astype(jnp.float32)
    inverse = lax.rsqrt(jnp.mean(floats * floats, axis=-1, keepdims=True) + norm_eps)
    return (floats * inverse * scaling).astype(jnp.bfloat16)


def stick_block(queries, packed, shifting, carried, allowed):
    length, head_count, head_width = queries.shape
    key_part = packed[:, : head_count * head_width].reshape(length, head_count, head_width)
    value_part = packed[:, head_count * head_width :].reshape(length, head_count, head_width)
    scores = jnp.einsum("thd,shd->hts", queries, key_part, preferred_element_type=jnp.float32)
    scores = scores * head_width ** (-0.5) + shifting[:, None, :]
    log_stay = jnp.where(allowed, jax.nn.log_sigmoid(-scores), 0.0)
    between = lax.cumsum(log_stay, axis=2, reverse=True) - log_stay
    weights = jnp.where(
        allowed, jnp.exp(jax.nn.log_sigmoid(scores) + between + carried[:, :, None]), 0.0
    )
    contrib = jnp.einsum(
        "hts,shd->thd", weights.astype(jnp.bfloat16), value_part, preferred_element_type=jnp.float32
    )
    return (contrib, carried + jnp.sum(log_stay, axis=2))


def per_device(
    mixer_rows,
    mixer_gain,
    w_query,
    w_key,
    w_value,
    key_shift,
    w_out,
    expert_rows,
    expert_gain,
    routes,
    route_weight,
    w_gate,
    w_up,
    w_down,
):
    length = mixer_rows.shape[0]
    head_count = key_shift.shape[0]
    head_width = w_query.shape[1] // head_count
    normed = rms_scale(mixer_rows, mixer_gain)
    queries = jnp.dot(normed, w_query, preferred_element_type=jnp.float32).astype(jnp.bfloat16)
    key_rows = jnp.dot(normed, w_key, preferred_element_type=jnp.float32).astype(jnp.bfloat16)
    value_rows = jnp.dot(normed, w_value, preferred_element_type=jnp.float32).astype(jnp.bfloat16)
    queries = queries.reshape(length, head_count, head_width)
    packed = jnp.concatenate([key_rows, value_rows], axis=1)
    device = lax.axis_index("ep")
    positions = jnp.arange(length, dtype=jnp.int32)
    strict = (positions[None, :] < positions[:, None])[None]
    own_shift = lax.dynamic_slice_in_dim(key_shift, device * length, length, 1)
    summed, carried = stick_block(
        queries, packed, own_shift, jnp.zeros((head_count, length), jnp.float32), strict
    )
    gathered = lax.all_gather(packed, "ep", axis=0, tiled=True)

    def visiting(offset, status):
        running, carry_now = status
        anchor = device - offset
        block_rows = lax.dynamic_slice_in_dim(gathered, anchor * length, length, 0)
        shifting = lax.dynamic_slice_in_dim(key_shift, anchor * length, length, 1)
        contrib, carry_now = stick_block(queries, block_rows, shifting, carry_now, True)
        return (running + contrib, carry_now)

    summed, carried = lax.fori_loop(1, device + 1, visiting, (summed, carried))
    head_out = summed.reshape(length, head_count * head_width).astype(jnp.bfloat16)
    weight_rows = w_out
    mixer_out = jnp.dot(
        lax.all_gather(head_out, "tp", axis=1, tiled=True),
        weight_rows,
        preferred_element_type=jnp.float32,
    ).astype(jnp.bfloat16)
    tokens_here, top_count = routes.shape
    expert_count = lax.axis_size("ep")
    capacity = 2 * tokens_here * top_count // expert_count
    rows_after_norm = rms_scale(expert_rows, expert_gain)
    chosen = routes.reshape(-1)
    hit_table = (chosen[:, None] == jnp.arange(expert_count, dtype=jnp.int32)[None, :]).astype(
        jnp.int32
    )
    places = jnp.sum((jnp.cumsum(hit_table, axis=0) - 1) * hit_table, axis=1)
    targets = chosen * capacity + places
    assign_ids = jnp.arange(tokens_here * top_count, dtype=jnp.int32) // top_count
    owners = (
        jnp.full((expert_count * capacity,), tokens_here, jnp.int32).at[targets].set(assign_ids)
    )
    padded = jnp.concatenate(
        [rows_after_norm, jnp.zeros((1, rows_after_norm.shape[1]), jnp.bfloat16)], axis=0
    )
    outgoing = padded[owners].reshape(expert_count, capacity, rows_after_norm.shape[1])
    gate_cols = w_gate[0]
    upper_cols = w_up[0]
    down_rows = w_down[0]
    arrived = lax.all_to_all(outgoing, "ep", split_axis=0, concat_axis=0, tiled=True)
    expert_senders, slots_here, feature_count = arrived.shape
    flat_rows = arrived.reshape(expert_senders * slots_here, feature_count)
    gating = jnp.minimum(
        jnp.dot(flat_rows, gate_cols, preferred_element_type=jnp.float32), glu_limit
    )
    linear = jnp.clip(
        jnp.dot(flat_rows, upper_cols, preferred_element_type=jnp.float32), -glu_limit, glu_limit
    )
    hidden = gating * jax.nn.sigmoid(glu_alpha * gating) * (linear + 1.0)
    hidden = hidden.astype(jnp.bfloat16).reshape(expert_senders, slots_here, gate_cols.shape[1])
    senders = hidden.shape[0]
    slot_total = hidden.shape[1]
    portion_units = lax.all_gather(hidden, "tp", axis=2, tiled=True)
    weight_rows = down_rows
    flat_units = portion_units.reshape(senders * slot_total, portion_units.shape[2])
    results = jnp.dot(flat_units, weight_rows, preferred_element_type=jnp.float32)
    leaving = results.astype(jnp.bfloat16).reshape(senders, slot_total, down_rows.shape[1])
    returned = lax.all_to_all(leaving, "ep", split_axis=0, concat_axis=0, tiled=True)
    picked = returned.reshape(expert_count * capacity, down_rows.shape[1])[targets].astype(
        jnp.float32
    )
    picked = picked * route_weight.reshape(-1)[:, None]
    expert_out = jnp.sum(picked.reshape(tokens_here, top_count, down_rows.shape[1]), axis=1).astype(
        jnp.bfloat16
    )
    return (mixer_out, expert_out)


def solution(mesh):
    placed = (
        P("ep", None),
        P(),
        P(None, "tp"),
        P(None, "tp"),
        P(None, "tp"),
        P("tp", None),
        P(None, "tp"),
        P("ep", None),
        P(),
        P("ep", None),
        P("ep", None),
        P("ep", None, "tp"),
        P("ep", None, "tp"),
        P("ep", None, "tp"),
    )
    return jax.shard_map(
        per_device,
        mesh=mesh,
        in_specs=placed,
        out_specs=(P("ep", "tp"), P("ep", "tp")),
        check_vma=False,
    )
```

profile of v0, /device:TPU:27, one launch (start us, length us, event | category | flops | bytes accessed | tf_op | source)
XLA Modules:
  0.0 386.4 jit_solution(7501015520184815229)
XLA Ops:
  7.2 0.9 copy.30
  9.1 1.1 reduce-window.26
  10.8 2.4 scatter_custom_fusion
  13.3 1.2 fusion.27
  14.5 1.2 fusion.29
  15.8 6.0 %gather_fusion = bf16[1024,2048]{1,0:T(8,128)(2,1)} fusion(bf16[129,2048]{1,0:T(8,128)(2,1)S(1)} %concatenate.7, s32[1024]{0:T(1024)S(1)} %fusion.40), kind=kCustom, calls=%fused_computation | custom fusion | bytes 8392704 | tf_op jit(solution)/shard_map/gather | solution.py:101
  21.8 96.8 %all_to_all.10 = bf16[8,128,2048]{2,1,0:T(8,128)(2,1)S(1)} all-to-all(bf16[8,128,2048]{2,1,0:T(8,128)(2,1)} %bitcast.92), channel_id=1, replica_groups=mesh['ep'=8,'tp'=4] {'ep'}, dimensions={0} | all-to-all | bytes 8388608 | tf_op jit(solution)/shard_map/all_to_all | solution.py:105
  118.6 2.3 fusion.17
  121.0 3.8 multiply_convert_fusion
  125.5 1.9 convolution_convert_fusion.1
  129.6 2.6 convolution_convert_fusion.2
  132.1 1.4 fusion.37
  133.5 1.3 fusion.49
  134.8 9.4 %fusion.35 = f32[4,256,2,128]{1,2,3,0:T(2,128)S(1)} fusion(f32[4,256,2,128]{1,3,2,0:T(8,128)S(1)} %bitcast.96), kind=kOutput, calls=%fused_computation.59 | output fusion | flops 33292288 | bytes 2097152 | tf_op jit(solution)/shard_map/reduce-window.2
  144.7 1.2 copy.27
  145.9 0.7 copy.32
  147.2 2.7 fusion.34
  150.1 27.8 %all-gather.5.cloned.1.call-done = bf16[8,128,2048]{2,1,0:T(8,128)(2,1)} async-done(((bf16[8,128,512]{2,1,0:T(8,128)(2,1)}), bf16[8,128,2048]{2,1,0:T(8,128)(2,1)}) %all-gather.5.cloned.1.call-update) | async-done | bytes 4194320 | tf_op jit(solution)/shard_map/all_gather | solution.py:118
  178.0 6.2 %fusion.23 = bf16[1024,512]{1,0:T(8,128)(2,1)} fusion(bf16[1024,2048]{1,0:T(8,128)(2,1)} %bitcast.105, bf16[1,2048,512]{2,1,0:T(8,128)(2,1)} %param.29), kind=kOutput, calls=%fused_computation.38 | convolution fusion | flops 2148007936 | bytes 7340032 | tf_op jit(solution)/shard_map/dot_general | solution.py:121
  184.2 5.5 %all-to-all-start.1 = ((bf16[8,128,512]{2,1,0:T(8,128)(2,1)}), bf16[8,128,512]{2,1,0:T(8,128)(2,1)}, u32[]{:S(2)}, u32[]{:S(2)}) async-start(bf16[8,128,512]{2,1,0:T(8,128)(2,1)} %bitcast.26), calls=%async_computation.1 | async-start | bytes 2097152 | tf_op jit(solution)/shard_map/all_to_all | solution.py:123
  189.7 38.2 %all-gather.3.cloned.1.call-done = bf16[2048,512]{0,1:T(8,128)(2,1)} async-done(((bf16[256,512]{0,1:T(8,128)(2,1)}), bf16[2048,512]{0,1:T(8,128)(2,1)}) %all-gather.3.cloned.1.call-update) | async-done | bytes 2097168 | tf_op jit(solution)/shard_map/all_gather | solution.py:66
  228.0 133.9 %while.12 = (s32[]{:T(128)}, f32[256,4,64]{0,2,1:T(8,128)S(1)}, f32[4,256]{1,0:T(4,128)}, s32[]{:T(128)}, s32[]{:T(128)}, /*index=5*/bf16[2048,512]{0,1:T(8,128)...) while((s32[]{:T(128)}, f32[256,4,64]{0,2,1:T(8,128)S(1)}, ...), condition=%wide.region_8.9_spmd, body=%wide.region_4.8_spmd.sunk | while | flops 108335112 | bytes 17314124 | solution.py:76
  228.0 1.0 constant_dynamic-slice_fusion.5
  229.6 3.4 fusion.80
  233.1 9.2 %fusion.81 = f32[4,256,2,128]{1,2,3,0:T(2,128)S(1)} fusion(f32[4,256,2,128]{1,3,2,0:T(8,128)S(1)} %bitcast.91), kind=kOutput, calls=%fused_computation.16.clone.1 | output fusion | flops 33292288 | bytes 2097152 | tf_op jit(solution)/shard_map/reduce-window
  242.9 0.7 reduce-window.39
  244.1 0.7 copy-done.1
  244.8 1.4 fusion.82
  247.1 1.0 constant_dynamic-slice_fusion.5
  248.7 3.4 fusion.80
  252.2 9.2 %fusion.81 = f32[4,256,2,128]{1,2,3,0:T(2,128)S(1)} fusion(f32[4,256,2,128]{1,3,2,0:T(8,128)S(1)} %bitcast.91), kind=kOutput, calls=%fused_computation.16.clone.1 | output fusion | flops 33292288 | bytes 2097152 | tf_op jit(solution)/shard_map/reduce-window
  262.0 0.7 reduce-window.39
  263.2 0.7 copy-done.1
  263.9 1.4 fusion.82
  266.1 1.0 constant_dynamic-slice_fusion.5
  267.8 3.4 fusion.80
  271.2 9.2 %fusion.81 = f32[4,256,2,128]{1,2,3,0:T(2,128)S(1)} fusion(f32[4,256,2,128]{1,3,2,0:T(8,128)S(1)} %bitcast.91), kind=kOutput, calls=%fused_computation.16.clone.1 | output fusion | flops 33292288 | bytes 2097152 | tf_op jit(solution)/shard_map/reduce-window
  281.0 0.7 reduce-window.39
  283.0 1.4 fusion.82
  285.2 1.0 constant_dynamic-slice_fusion.5
  286.9 3.4 fusion.80
  290.3 9.2 %fusion.81 = f32[4,256,2,128]{1,2,3,0:T(2,128)S(1)} fusion(f32[4,256,2,128]{1,3,2,0:T(8,128)S(1)} %bitcast.91), kind=kOutput, calls=%fused_computation.16.clone.1 | output fusion | flops 33292288 | bytes 2097152 | tf_op jit(solution)/shard_map/reduce-window
  300.1 0.7 reduce-window.39
  302.1 1.4 fusion.82
  304.3 1.0 constant_dynamic-slice_fusion.5
  306.0 3.4 fusion.80
  309.4 9.2 %fusion.81 = f32[4,256,2,128]{1,2,3,0:T(2,128)S(1)} fusion(f32[4,256,2,128]{1,3,2,0:T(8,128)S(1)} %bitcast.91), kind=kOutput, calls=%fused_computation.16.clone.1 | output fusion | flops 33292288 | bytes 2097152 | tf_op jit(solution)/shard_map/reduce-window
  319.2 0.7 reduce-window.39
  321.2 1.4 fusion.82
  323.4 1.0 constant_dynamic-slice_fusion.5
  325.1 3.4 fusion.80
  328.5 9.2 %fusion.81 = f32[4,256,2,128]{1,2,3,0:T(2,128)S(1)} fusion(f32[4,256,2,128]{1,3,2,0:T(8,128)S(1)} %bitcast.91), kind=kOutput, calls=%fused_computation.16.clone.1 | output fusion | flops 33292288 | bytes 2097152 | tf_op jit(solution)/shard_map/reduce-window
  338.3 0.7 reduce-window.39
  340.3 1.4 fusion.82
  342.5 1.0 constant_dynamic-slice_fusion.5
  344.2 3.4 fusion.80
  347.6 9.2 %fusion.81 = f32[4,256,2,128]{1,2,3,0:T(2,128)S(1)} fusion(f32[4,256,2,128]{1,3,2,0:T(8,128)S(1)} %bitcast.91), kind=kOutput, calls=%fused_computation.16.clone.1 | output fusion | flops 33292288 | bytes 2097152 | tf_op jit(solution)/shard_map/reduce-window
  357.4 0.7 reduce-window.39
  359.4 1.4 fusion.82
  361.9 8.1 %all_gather.10 = bf16[256,1024]{0,1:T(8,128)(2,1)S(1)} all-gather(bf16[256,256]{0,1:T(8,128)(2,1)S(1)} %bitcast.99), channel_id=1, replica_groups=mesh['ep'=8,'tp'=4] {'tp'}, dimensions={1}, use_global_device_ids=true | all-gather | bytes 655360 | tf_op jit(solution)/shard_map/all_gather | solution.py:80
  369.9 2.4 convolution_convert_fusion
  372.3 4.1 %gather_fusion.1 = bf16[512,512]{1,0:T(8,128)(2,1)} fusion(bf16[1024,512]{1,0:T(8,128)(2,1)} %bitcast.27, s32[1024]{0:T(1024)S(1)} %copy-done.9), kind=kCustom, calls=%fused_computation.1 | custom fusion | bytes 1050624 | tf_op jit(solution)/shard_map/gather | solution.py:124
  376.4 1.4 reshape.162
  377.8 1.4 multiply_reduce_fusion
  (156 shorter events, 27.3 us)
Async XLA Ops:
  7.2 111.4 %copy-start = (bf16[1,2048,512]{2,1,0:T(8,128)(2,1)S(1)}, bf16[1,2048,512]{2,1,0:T(8,128)(2,1)}, u32[]{:S(2)}) copy-start(bf16[1,2048,512]{2,1,0:T(8,128)(2,1)} %param.28) | copy-start | bytes 6291460
  7.2 170.8 %all-gather.5.cloned.1.call-start = ((), (), s32[]{:S(2)}) async-start(), calls=%async_computation.3 | async-start | bytes 5242880 | tf_op jit(solution)/shard_map/all_gather | solution.py:118
  118.6 2.4 copy-start.11
  121.0 4.1 %copy-start.4 = (bf16[256,2048]{1,0:T(8,128)(2,1)S(1)}, bf16[256,2048]{1,0:T(8,128)(2,1)}, u32[]{:S(2)}) copy-start(bf16[256,2048]{1,0:T(8,128)(2,1)} %param.16) | copy-start | bytes 3145732
  124.8 0.7 copy-start.13
  124.8 103.1 %all-gather.3.cloned.1.call-start = ((), (), s32[]{:S(2)}) async-start(), calls=%async_computation.2 | async-start | bytes 2359296 | tf_op jit(solution)/shard_map/all_gather | solution.py:66
  125.1 2.3 copy-start.12
  133.5 1.3 copy-start.2
  144.3 1.6 copy-start.10
  144.7 2.5 copy-start.3
  184.2 188.1 %all-to-all-start.1 = ((bf16[8,128,512]{2,1,0:T(8,128)(2,1)}), bf16[8,128,512]{2,1,0:T(8,128)(2,1)}, u32[]{:S(2)}, u32[]{:S(2)}) async-start(bf16[8,128,512]{2,1,0:T(8,128)(2,1)} %bitcast.26), calls=%async_computation.1 | async-start | bytes 2097152 | tf_op jit(solution)/shard_map/all_to_all | solution.py:123
  243.6 1.2 copy-start.1
  243.6 1.2 copy-start.5
  244.1 2.3 copy-start.8
  246.5 0.6 copy-start.6
  262.7 1.2 copy-start.1
  262.7 1.2 copy-start.5
  263.2 2.3 copy-start.8
  265.6 0.6 copy-start.6
  281.8 1.2 copy-start.1
  281.8 1.2 copy-start.5
  282.3 2.3 copy-start.8
  284.6 0.6 copy-start.6
  300.9 1.2 copy-start.1
  300.9 1.2 copy-start.5
  301.4 2.3 copy-start.8
  303.7 0.6 copy-start.6
  320.0 1.2 copy-start.1
  320.0 1.2 copy-start.5
  320.5 2.3 copy-start.8
  322.8 0.6 copy-start.6
  339.1 1.2 copy-start.1
  339.1 1.2 copy-start.5
  339.6 2.3 copy-start.8
  341.9 0.6 copy-start.6
  358.2 1.2 copy-start.1
  358.2 1.2 copy-start.5
  358.6 2.3 copy-start.8
  361.0 0.6 copy-start.6
  361.8 10.5 %copy-start.9 = (s32[1024]{0:T(1024)S(1)}, s32[1024]{0:T(1024)}, u32[]{:S(2)}) copy-start(s32[1024]{0:T(1024)} %pad_clamp_fusion) | copy-start | bytes 12292
  372.3 5.4 %copy-start.7 = (f32[128,4]{1,0:T(8,128)S(1)}, f32[128,4]{1,0:T(8,128)}, u32[]{:S(2)}) copy-start(f32[128,4]{1,0:T(8,128)} %copy.32) | copy-start | bytes 6148
Sparse Core Ops, SparseCore 0:
  125.0 52.9 all-gather.4
  180.1 47.7 all-gather.2
where the time goes:
time: 393 us; the launch traced here: 386 us
  blocking collectives  105 us (27%)
  other arithmetic  103 us (26%)
  waiting for transfers between devices  66.1 us (17%)
  matrix products  46.9 us (12%)
  local copies, waits for them, and re-layouts  44.1 us (11%)
  between operations  14.7 us (4%)
  starting transfers between devices  5.8 us (1%)
    all_to_all x1, blocking collectives, per_device(): lax.all_to_all(outgoing, 'ep', split_axis=0, concat_axis=0, tiled=True)  96.8 us
    another operation x18, other arithmetic  80.1 us
    all_gather x1, waiting for transfers between devices, per_device(): gathered = lax.all_gather(packed, 'ep', axis=0, tiled=True)  38.2 us
    all_gather x1, waiting for transfers between devices, per_device(): portion_units = lax.all_gather(hidden, 'tp', axis=2, tiled=True)  27.8 us
    dot_general x8, matrix products, stick_block(): jnp.einsum('thd,shd->hts', queries, key_part, preferred_element_type=jnp....  25.3 us
    convert_element_type x8, other arithmetic, stick_block(): weights.astype(jnp.bfloat16)  12.4 us
    while x56, local copies, waits for them, and re-layouts  9.15 us
    all_gather x1, blocking collectives, per_device(): lax.all_gather(head_out, 'tp', axis=1, tiled=True)  8.07 us
  transfers between devices with their start and end apart: 3, of which 2 were waited for; matrix products, arithmetic and copies ran while one was open for 41% of the time, Pallas kernels for 0%

commit v1 on v0

v1 whole, which is shorter than its diff:
```python
import functools

import jax
import jax.numpy as jnp
from jax import lax
from jax.experimental import pallas as pl
from jax.experimental.pallas import tpu as pltpu
from jax.sharding import PartitionSpec as P

norm_eps = 1e-06
glu_limit = 7.0
glu_alpha = 1.702


def rms_scale(source, scaling):
    floats = source.astype(jnp.float32)
    inverse = lax.rsqrt(jnp.mean(floats * floats, axis=-1, keepdims=True) + norm_eps)
    return (floats * inverse * scaling).astype(jnp.bfloat16)


def stick_kernel(device_ref, q_ref, kv_ref, shift_ref, out_ref, acc_ref, carry_ref, *, head_count):
    length, columns = q_ref.shape
    width = columns // head_count
    device = device_ref[0]
    row = lax.broadcasted_iota(jnp.int32, (length, length), 0)
    col = lax.broadcasted_iota(jnp.int32, (length, length), 1)
    later = (row >= col).astype(jnp.bfloat16)
    strict = col < row
    scale = width ** (-0.5)

    def visit(block, first):
        start = pl.multiple_of(block * length, length)
        shifting = shift_ref[:, pl.ds(start, length)]
        for head in range(head_count):
            low, high = head * width, (head + 1) * width
            key_part = kv_ref[pl.ds(start, length), low:high]
            value_part = kv_ref[pl.ds(start, length), columns + low : columns + high]
            scores = lax.dot_general(
                q_ref[:, low:high],
                key_part,
                (((1,), (1,)), ((), ())),
                preferred_element_type=jnp.float32,
            )
            scores = scores * scale + shifting[head : head + 1, :]
            leave = jnp.maximum(scores, 0.0) + jnp.log(1.0 + jnp.exp(-jnp.abs(scores)))
            if first:
                leave = jnp.where(strict, leave, 0.0)
            coarse = leave.astype(jnp.bfloat16)
            fine = (leave - coarse.astype(jnp.float32)).astype(jnp.bfloat16)
            onward = jnp.dot(coarse, later, preferred_element_type=jnp.float32) + jnp.dot(
                fine, later, preferred_element_type=jnp.float32
            )
            if first:
                weights = jnp.where(strict, jnp.exp(scores - onward), 0.0)
                carry_ref[head] = onward[:, 0:1]
            else:
                carried = carry_ref[head]
                weights = jnp.exp(scores - onward - carried)
                carry_ref[head] = carried + onward[:, 0:1]
            contrib = jnp.dot(
                weights.astype(jnp.bfloat16), value_part, preferred_element_type=jnp.float32
            )
            if first:
                acc_ref[:, low:high] = contrib
            else:
                acc_ref[:, low:high] += contrib

    visit(device, True)

    @pl.loop(0, device)
    def _(step):
        visit(device - 1 - step, False)

    out_ref[...] = acc_ref[...].astype(jnp.bfloat16)


def stick_attention(device, queries, gathered, key_shift):
    length, columns = queries.shape
    head_count = key_shift.shape[0]
    vmem = pl.BlockSpec(memory_space=pltpu.VMEM)
    return pl.pallas_call(
        functools.partial(stick_kernel, head_count=head_count),
        in_specs=[pl.BlockSpec(memory_space=pltpu.SMEM), vmem, vmem, vmem],
        out_specs=vmem,
        out_shape=jax.ShapeDtypeStruct((length, columns), jnp.bfloat16),
        scratch_shapes=[
            pltpu.VMEM((length, columns), jnp.float32),
            pltpu.VMEM((head_count, length, 1), jnp.float32),
        ],
        cost_estimate=pl.CostEstimate(
            flops=8 * head_count * length * gathered.shape[0] * length,
            transcendentals=3 * head_count * length * gathered.shape[0],
            bytes_accessed=2 * gathered.size,
        ),
        name="stick_attention",
    )(device.reshape(1), queries, gathered, key_shift)


def per_device(
    mixer_rows,
    mixer_gain,
    w_query,
    w_key,
    w_value,
    key_shift,
    w_out,
    expert_rows,
    expert_gain,
    routes,
    route_weight,
    w_gate,
    w_up,
    w_down,
):
    tp_count = lax.axis_size("tp")
    ep_count = lax.axis_size("ep")
    tokens_here, top_count = routes.shape
    share = tokens_here // tp_count
    own_rows = lax.dynamic_slice_in_dim(expert_rows, lax.axis_index("tp") * share, share, 0)
    all_rows = lax.all_gather(
        rms_scale(own_rows, expert_gain), ("ep", "tp"), axis=0, tiled=True
    )

    normed = rms_scale(mixer_rows, mixer_gain)
    key_rows = jnp.dot(normed, w_key, preferred_element_type=jnp.float32).astype(jnp.bfloat16)
    value_rows = jnp.dot(normed, w_value, preferred_element_type=jnp.float32).astype(jnp.bfloat16)
    packed = jnp.concatenate([key_rows, value_rows], axis=1)
    gathered = lax.all_gather(packed, "ep", axis=0, tiled=True)
    queries = jnp.dot(normed, w_query, preferred_element_type=jnp.float32).astype(jnp.bfloat16)

    gating = jnp.minimum(
        jnp.dot(all_rows, w_gate[0], preferred_element_type=jnp.float32), glu_limit
    )
    linear = jnp.clip(
        jnp.dot(all_rows, w_up[0], preferred_element_type=jnp.float32), -glu_limit, glu_limit
    )
    hidden = (gating * jax.nn.sigmoid(glu_alpha * gating) * (linear + 1.0)).astype(jnp.bfloat16)
    units = lax.all_gather(hidden, "tp", axis=1, tiled=True)

    device = lax.axis_index("ep").astype(jnp.int32)
    head_out = stick_attention(device, queries, gathered, key_shift)
    mixer_out = jnp.dot(
        lax.all_gather(head_out, "tp", axis=1, tiled=True),
        w_out,
        preferred_element_type=jnp.float32,
    ).astype(jnp.bfloat16)

    results = jnp.dot(units, w_down[0], preferred_element_type=jnp.float32).astype(jnp.bfloat16)
    leaving = results.reshape(ep_count, tokens_here, results.shape[1])
    returned = lax.all_to_all(leaving, "ep", split_axis=0, concat_axis=0, tiled=True)
    named = routes[None] == jnp.arange(ep_count, dtype=jnp.int32)[:, None, None]
    shares = jnp.sum(jnp.where(named, route_weight[None], 0.0), axis=2)
    expert_out = jnp.sum(returned.astype(jnp.float32) * shares[:, :, None], axis=0).astype(
        jnp.bfloat16
    )
    return (mixer_out, expert_out)


def solution(mesh):
    placed = (
        P("ep", None),
        P(),
        P(None, "tp"),
        P(None, "tp"),
        P(None, "tp"),
        P("tp", None),
        P(None, "tp"),
        P("ep", None),
        P(),
        P("ep", None),
        P("ep", None),
        P("ep", None, "tp"),
        P("ep", None, "tp"),
        P("ep", None, "tp"),
    )
    return jax.shard_map(
        per_device,
        mesh=mesh,
        in_specs=placed,
        out_specs=(P("ep", "tp"), P("ep", "tp")),
        check_vma=False,
    )
```

time: 393 us -> 225 us (0.57); the launches traced: 386 us -> 225 us
  other arithmetic: 103 us -> 4.82 us
  blocking collectives: 105 us -> 13.3 us
  waiting for transfers between devices: 66.1 us -> 146 us
  local copies, waits for them, and re-layouts: 44.1 us -> 0.34 us
  matrix products: 46.9 us -> 22 us
  Pallas kernels: 0 us -> 18.3 us
    all_to_all x1 -> x0, blocking collectives: 96.8 us -> none  [per_device(): lax.all_to_all(outgoing, 'ep', split_axis=0, concat_axis=0, tiled=True)]
    all_gather x1 -> x2, waiting for transfers between devices: 27.8 us -> 112 us  [the longest x1 62.9 us: per_device(): lax.all_gather(rms_scale(own_rows, expert_gain), ('ep', 'tp'), axis=0, ti...]
    another operation x26 -> x0, other arithmetic: 83.1 us -> none
    dot_general x20 -> x4, matrix products: 41.8 us -> 17.1 us  [the longest x1 6.19 us: per_device(): jnp.dot(units, w_down[0], preferred_element_type=jnp.float32)]
    pallas_call x0 -> x1, Pallas kernels: none -> 18.3 us  [stick_attention(): pl.pallas_call(functools.partial(stick_kernel, head_count=head_count), in...]
    convert_element_type x10 -> x0, other arithmetic: 12.4 us -> none  [the longest x8 12.4 us: stick_block(): weights.astype(jnp.bfloat16)]
    gather x2 -> x0, local copies, waits for them, and re-layouts: 10.1 us -> none  [the longest x1 6.02 us: per_device(): padded[owners].reshape(expert_count, capacity, rows_after_norm.shape[1])]
    while x56 -> x0, local copies, waits for them, and re-layouts: 9.15 us -> none
  transfers between devices with their start and end apart: 3 -> 4, of which waited for: 2 -> 3; matrix products, arithmetic and copies ran while one was open for 41% -> 6% of each run, Pallas kernels for 0% -> 8%
where the time goes in v1:
time: 225 us
  waiting for transfers between devices  146 us (65%)
  matrix products  22 us (10%)
  Pallas kernels  18.3 us (8%)
  between operations  13.8 us (6%)
  blocking collectives  13.3 us (6%)
  starting transfers between devices  5.82 us (3%)
  other arithmetic  4.82 us (2%)
    all_gather x1, waiting for transfers between devices, per_device(): lax.all_gather(rms_scale(own_rows, expert_gain), ('ep', 'tp'), axis=0, ti...  62.9 us
    all_gather x1, waiting for transfers between devices, per_device(): units = lax.all_gather(hidden, 'tp', axis=1, tiled=True)  48.6 us
    all_gather x1, waiting for transfers between devices, per_device(): gathered = lax.all_gather(packed, 'ep', axis=0, tiled=True)  34.6 us
    pallas_call x1, Pallas kernels, stick_attention(): pl.pallas_call(functools.partial(stick_kernel, head_count=head_count), in...  18.3 us
    all_gather x1, blocking collectives, per_device(): lax.all_gather(head_out, 'tp', axis=1, tiled=True)  13.3 us
    dot_general x1, matrix products, per_device(): jnp.dot(units, w_down[0], preferred_element_type=jnp.float32)  6.19 us
    all_to_all x1, starting transfers between devices, per_device(): lax.all_to_all(leaving, 'ep', split_axis=0, concat_axis=0, tiled=True)  5.7 us
    dot_general x1, matrix products, per_device(): jnp.dot(all_rows, w_up[0], preferred_element_type=jnp.float32)  4.67 us
  transfers between devices with their start and end apart: 4, of which 3 were waited for; matrix products, arithmetic and copies ran while one was open for 6% of the time, Pallas kernels for 8%

profile of v1, /device:TPU:27, one launch (start us, length us, event | category | flops | bytes accessed | tf_op | source)
XLA Modules:
  0.0 224.6 jit_solution(5010900692831373732)
XLA Ops:
  7.2 0.0 copy-start
  7.2 0.0 all-gather.6.cloned.1.call-start
  7.2 1.2 fusion.14
  8.4 1.7 fusion.16
  10.1 0.0 all-gather.6.cloned.1.call-update
  10.1 0.0 all-gather.8.cloned.1.call-start
  10.2 62.9 %all-gather.6.cloned.1.call-done = bf16[1024,2048]{1,0:T(8,128)(2,1)} async-done(((bf16[32,2048]{1,0:T(8,128)(2,1)}), bf16[1024,2048]{1,0:T(8,128)(2,1)}) %all-gather.6.cloned.1.call-update) | async-done | bytes 4194320 | tf_op jit(solution)/shard_map/all_gather | solution.py:120
  73.1 0.0 copy-done
  73.1 0.0 copy-start.4
  73.1 0.0 copy-start.5
  73.1 4.7 %fusion.5 = f32[1024,512]{1,0:T(8,128)S(1)} fusion(bf16[1024,2048]{1,0:T(8,128)(2,1)} %all-gather.6.cloned.1.call-done, bf16[1,2048,512]{2,1,0:T(8,128)(2,1)S(1)} %copy-done), kind=kOutput, calls=%fused_computation.7 | convolution fusion | flops 2147483648 | bytes 8388608 | tf_op jit(solution)/shard_map/dot_general | solution.py:135
  77.8 0.0 copy-done.4
  77.8 0.0 copy-done.5
  77.8 0.0 copy-start.1
  77.8 3.8 %multiply_convert_fusion = bf16[1024,512]{1,0:T(8,128)(2,1)} fusion(f32[1024,512]{1,0:T(8,128)S(1)} %fusion.5, bf16[1024,2048]{1,0:T(8,128)(2,1)S(1)} %copy-done.4, bf16[1,2048,512]{2,1,0:T(8,128)(2,1)S(1)} %copy-done.5), kind=kOutput, calls=%fused_computation.12 | convolution fusion | flops 2152726528 | bytes 9437184 | tf_op jit(solution)/shard_map/dot_general | solution.py:132
  81.6 0.0 copy-start.7
  81.6 0.0 all-gather.8.cloned.1.call-update
  81.7 0.0 all-gather.4.cloned.1.call-start
  81.7 0.0 copy-done.1
  81.7 0.0 copy-start.6
  81.7 0.3 fusion
  82.0 0.3 copy-done.7
  82.3 1.7 convolution_convert_fusion.1
  84.1 0.0 copy-done.6
  84.1 0.5 convolution_convert_fusion.2
  84.6 0.7 pad_maximum_fusion
  85.3 0.0 all-gather.4.cloned.1.call-update
  85.3 48.6 %all-gather.8.cloned.1.call-done = bf16[1024,2048]{1,0:T(8,128)(2,1)} async-done(((bf16[1024,512]{1,0:T(8,128)(2,1)}), bf16[1024,2048]{1,0:T(8,128)(2,1)}) %all-gather.8.cloned.1.call-update) | async-done | bytes 4194320 | tf_op jit(solution)/shard_map/all_gather | solution.py:138
  133.9 6.2 %fusion.11 = bf16[1024,512]{1,0:T(8,128)(2,1)} fusion(bf16[1024,2048]{1,0:T(8,128)(2,1)} %all-gather.8.cloned.1.call-done, bf16[1,2048,512]{2,1,0:T(8,128)(2,1)} %param.27), kind=kOutput, calls=%fused_computation.13 | convolution fusion | flops 2148007936 | bytes 7340032 | tf_op jit(solution)/shard_map/dot_general | solution.py:148
  140.1 0.0 copy-start.2
  140.1 0.0 copy-start.3
  140.1 5.7 %all-to-all-start = ((bf16[8,128,512]{2,1,0:T(8,128)(2,1)}), bf16[8,128,512]{2,1,0:T(8,128)(2,1)S(1)}, u32[]{:S(2)}, u32[]{:S(2)}) async-start(bf16[8,128,512]{2,1,0:T(8,128)(2,1)} %bitcast.23), calls=%async_computation | async-start | bytes 2097152 | tf_op jit(solution)/shard_map/all_to_all | solution.py:150
  145.8 0.0 copy-done.2
  145.8 0.0 copy-done.3
  145.8 2.7 %convolution_convert_fusion.3.q_ref = bf16[256,256]{1,0:T(8,128)(2,1)} fusion(bf16[2048,256]{1,0:T(8,128)(2,1)} %param.16, bf16[256,2048]{1,0:T(8,128)(2,1)} %param.14, f32[2048]{0:T(1024)S(1)} %copy-done.7, f32[256]{0:T(256)S(1)} %add_rsqrt_fusion), kind=kOutput, calls=%fused_computation.17 | convolution fusion | flops 270598144 | bytes 2237440 | tf_op jit(solution)/shard_map/dot_general | solution.py:129
  148.5 34.6 %all-gather.4.cloned.1.call-done.kv_ref = bf16[2048,512]{1,0:T(8,128)(2,1)} async-done(((bf16[256,512]{1,0:T(8,128)(2,1)}), bf16[2048,512]{1,0:T(8,128)(2,1)}) %all-gather.4.cloned.1.call-update) | async-done | bytes 2097168 | tf_op jit(solution)/shard_map/all_gather | solution.py:128
  183.1 18.3 %stick_attention.1 = bf16[256,256]{1,0:T(8,128)(2,1)} custom-call(s32[1]{0:T(128)} %bitcast.device_ref, bf16[256,256]{1,0:T(8,128)(2,1)} %convolution_convert_fusion.3.q_ref, bf16[2048,512]{1,0:T(8,128)(2,1)} %all-gather.4.cloned.1.call-done.kv_ref, f32[4,2048]{1,0:T(4,128)} %shift_ref.1), custom_call_target="tpu_custom_call" | custom-call | flops 4294967296 | bytes 2097152 | tf_op jit(solution)/shard_map/stick_attention/pallas_call | solution.py:81
  201.4 13.3 %all_gather.13 = bf16[256,1024]{1,0:T(8,128)(2,1)S(1)} all-gather(bf16[256,256]{1,0:T(8,128)(2,1)} %stick_attention.1), channel_id=1, replica_groups=mesh['ep'=8,'tp'=4] {'tp'}, dimensions={1}, use_global_device_ids=true | all-gather | bytes 655360 | tf_op jit(solution)/shard_map/all_gather | solution.py:143
  214.7 2.4 %convolution_convert_fusion = bf16[256,512]{1,0:T(8,128)(2,1)} fusion(bf16[256,1024]{1,0:T(8,128)(2,1)S(1)} %all_gather.13, bf16[1024,512]{1,0:T(8,128)(2,1)} %param.20), kind=kOutput, calls=%fused_computation.14 | convolution fusion | flops 268566528 | bytes 1835008 | tf_op jit(solution)/shard_map/dot_general | solution.py:142
  217.1 0.0 all-to-all-done
  217.1 0.9 multiply_reduce_fusion
  (3 shorter events, 0.0 us)
Async XLA Ops:
  7.2 65.9 %copy-start = (bf16[1,2048,512]{2,1,0:T(8,128)(2,1)S(1)}, bf16[1,2048,512]{2,1,0:T(8,128)(2,1)}, u32[]{:S(2)}) copy-start(bf16[1,2048,512]{2,1,0:T(8,128)(2,1)} %param.26) | copy-start | bytes 6291460
  7.2 65.9 %all-gather.6.cloned.1.call-start = ((), (), s32[]{:S(2)}) async-start(), calls=%async_computation.2 | async-start | bytes 4325376 | tf_op jit(solution)/shard_map/all_gather | solution.py:120
  10.1 123.8 %all-gather.8.cloned.1.call-start = ((), (), s32[]{:S(2)}) async-start(), calls=%async_computation.3 | async-start | bytes 5242880 | tf_op jit(solution)/shard_map/all_gather | solution.py:138
  73.1 4.7 %copy-start.4 = (bf16[1024,2048]{1,0:T(8,128)(2,1)S(1)}, bf16[1024,2048]{1,0:T(8,128)(2,1)}, u32[]{:S(2)}) copy-start(bf16[1024,2048]{1,0:T(8,128)(2,1)} %all-gather.6.cloned.1.call-done) | copy-start | bytes 12582916
  73.1 4.7 %copy-start.5 = (bf16[1,2048,512]{2,1,0:T(8,128)(2,1)S(1)}, bf16[1,2048,512]{2,1,0:T(8,128)(2,1)}, u32[]{:S(2)}) copy-start(bf16[1,2048,512]{2,1,0:T(8,128)(2,1)} %param.25) | copy-start | bytes 6291460
  77.8 3.9 %copy-start.1 = (bf16[256,2048]{1,0:T(8,128)(2,1)S(1)}, bf16[256,2048]{1,0:T(8,128)(2,1)}, u32[]{:S(2)}) copy-start(bf16[256,2048]{1,0:T(8,128)(2,1)} %param.14) | copy-start | bytes 3145732
  81.6 0.7 copy-start.7
  81.7 101.5 %all-gather.4.cloned.1.call-start = ((), (), s32[]{:S(2)}) async-start(), calls=%async_computation.1 | async-start | bytes 2359296 | tf_op jit(solution)/shard_map/all_gather | solution.py:128
  81.7 2.3 %copy-start.6 = (bf16[2048,256]{1,0:T(8,128)(2,1)S(1)}, bf16[2048,256]{1,0:T(8,128)(2,1)}, u32[]{:S(2)}) copy-start(bf16[2048,256]{1,0:T(8,128)(2,1)} %param.17) | copy-start | bytes 3145732
  140.1 5.7 %copy-start.2 = (f32[128,4]{0,1:T(4,128)S(1)}, f32[128,4]{0,1:T(4,128)}, u32[]{:S(2)}) copy-start(f32[128,4]{0,1:T(4,128)} %param.24) | copy-start | bytes 6148
  140.1 5.7 %copy-start.3 = (s32[128,4]{0,1:T(4,128)S(1)}, s32[128,4]{0,1:T(4,128)}, u32[]{:S(2)}) copy-start(s32[128,4]{0,1:T(4,128)} %param.23) | copy-start | bytes 6148
  140.1 77.0 %all-to-all-start = ((bf16[8,128,512]{2,1,0:T(8,128)(2,1)}), bf16[8,128,512]{2,1,0:T(8,128)(2,1)S(1)}, u32[]{:S(2)}, u32[]{:S(2)}) async-start(bf16[8,128,512]{2,1,0:T(8,128)(2,1)} %bitcast.23), calls=%async_computation | async-start | bytes 2097152 | tf_op jit(solution)/shard_map/all_to_all | solution.py:150
Sparse Core Ops, SparseCore 0:
  11.4 61.6 all-gather.5
  81.8 52.0 all-gather.7
  136.1 47.0 all-gather.3
